TPU v7x, 32 devices: a whole 2x2x4 slice. The times are simulated.
32 devices in a mesh: rep: 4 (over z), fs: 4 (over y, x), tp: 2 (over core).
Axes of the slice: x: 2, y: 2, z: 4, core: 2. Of those that a mesh axis runs over, the one named last changes fastest.
Arguments:
- inputs: bfloat16 [512, 2048], P(('rep', 'fs', 'tp')), may hold values from -6 to 6
- cotangent: bfloat16 [512, 2048], P(('rep', 'fs', 'tp')), may hold values from -6 to 6
- norm_gain: float32 [2048], replicated, may hold values from 0.1 to 1.9
- gate_weight: bfloat16 [2048, 2816], P(None, ('fs', 'tp')), may hold values from -0.125 to 0.125
- up_weight: bfloat16 [2048, 2816], P(None, ('fs', 'tp')), may hold values from -0.125 to 0.125
- down_weight: bfloat16 [2816, 2048], P(('fs', 'tp')), may hold values from -0.109375 to 0.109375
Outputs:
- input_grad: bfloat16 [512, 2048], P(('rep', 'fs', 'tp'))
- gain_grad: float32 [2048], replicated
- down_grad: float32 [2816, 2048], P(('fs', 'tp'), 'rep')
All inputs are finite; a program needn't handle non-finite values.
Results may differ from a plain program's by a relative error of at most 0.0066.
Values may be sent and summed in bfloat16 or wider, within the bound.
A program may use at most 64 MiB of HBM per device.

v0:
```python
import jax
import jax.numpy as jnp
from jax import lax
from jax.sharding import PartitionSpec as P

EPS = 1e-06


def across_tokens(left, right):
    return lax.dot_general(
        left, right, (((0,), (0,)), ((), ())), preferred_element_type=jnp.float32
    )


def across_columns(left, right):
    return lax.dot_general(
        left, right, (((1,), (1,)), ((), ())), preferred_element_type=jnp.float32
    )


def per_device(inputs, cotangent, norm_gain, gate_weight, up_weight, down_weight):
    whole_x, whole_dy = (
        lax.all_gather(inputs, ("fs", "tp"), axis=0, tiled=True),
        lax.all_gather(cotangent, ("fs", "tp"), axis=0, tiled=True),
    )
    xf = whole_x.astype(jnp.float32)
    inv = lax.rsqrt(jnp.mean(xf * xf, axis=-1, keepdims=True) + EPS)
    normed = xf * inv
    hidden_in = (normed * norm_gain).astype(jnp.bfloat16)
    gate = jnp.dot(hidden_in, gate_weight, preferred_element_type=jnp.float32)
    up = jnp.dot(hidden_in, up_weight, preferred_element_type=jnp.float32)
    sig = jax.nn.sigmoid(gate)
    act = gate * sig
    hidden = (act * up).astype(jnp.bfloat16)
    d_hidden = 0.5 * across_columns(whole_dy, down_weight)
    d_gate = (d_hidden * up * sig * (1.0 + gate * (1.0 - sig))).astype(jnp.bfloat16)
    d_up = (d_hidden * act).astype(jnp.bfloat16)
    own_rows = inputs.shape[0]
    d_in = lax.psum_scatter(
        across_columns(d_gate, gate_weight) + across_columns(d_up, up_weight),
        ("fs", "tp"),
        scatter_dimension=0,
        tiled=True,
    )
    offset = lax.axis_index(("fs", "tp")) * own_rows
    own_normed = lax.dynamic_slice_in_dim(normed, offset, own_rows, 0)
    own_inv = lax.dynamic_slice_in_dim(inv, offset, own_rows, 0)
    gain_grad = lax.psum(jnp.sum(d_in * own_normed, axis=0), ("rep", "fs", "tp"))
    scaled = d_in * norm_gain
    input_grad = (
        own_inv * (scaled - own_normed * jnp.mean(scaled * own_normed, axis=-1, keepdims=True))
    ).astype(jnp.bfloat16)
    input_grad, gain_grad = (input_grad, gain_grad)
    part_down = 0.5 * across_tokens(whole_dy, hidden)
    got_down = lax.all_to_all(
        part_down[None].astype(jnp.bfloat16), "rep", split_axis=1, concat_axis=0, tiled=True
    ).astype(jnp.float32)
    down_grad = jnp.sum(got_down, axis=0).T
    return (input_grad, gain_grad, down_grad)


def solution(mesh):
    return jax.shard_map(
        per_device,
        mesh=mesh,
        in_specs=(
            P(("rep", "fs", "tp"), None),
            P(("rep", "fs", "tp"), None),
            P(),
            P(None, ("fs", "tp")),
            P(None, ("fs", "tp")),
            P(("fs", "tp"), None),
        ),
        out_specs=(P(("rep", "fs", "tp"), None), P(), P(("fs", "tp"), "rep")),
        check_vma=False,
    )
```

profile of v0, /device:TPU:0, one launch (start us, length us, event | category | flops | bytes accessed | tf_op | source)
XLA Modules:
  0.0 166.7 jit_solution(2304956729085242355)
XLA Ops:
  7.2 0.0 copy-start
  7.2 0.0 reduce-scatter.2.cloned.1.call-start
  7.2 11.8 %all_gather.6 = bf16[128,2048]{1,0:T(8,128)(2,1)S(1)} all-gather(bf16[16,2048]{1,0:T(8,128)(2,1)} %param.6), channel_id=1, replica_groups=mesh['rep'=4,'fs'=4,'tp'=2] {'fs','tp'}, dimensions={0}, use_global_device_ids=true | all-gather | bytes 589824 | tf_op jit(solution)/shard_map/all_gather | solution.py:23
  19.0 0.0 copy-start.4
  19.0 0.0 copy-start.7
  19.0 0.2 fusion.2
  19.2 0.0 copy-done
  19.2 1.4 fusion.3
  20.6 0.0 copy-done.4
  20.6 0.0 copy-done.7
  20.6 0.0 copy-start.2
  20.6 0.0 copy-start.6
  20.7 0.0 copy-start.3
  20.7 0.6 fusion.4
  21.3 0.3 copy-done.6
  21.6 0.0 copy-start.5
  21.6 9.5 %all_gather.7 = bf16[128,2048]{1,0:T(8,128)(2,1)S(1)} all-gather(bf16[16,2048]{1,0:T(8,128)(2,1)S(1)} %copy-done.6), channel_id=1, replica_groups=mesh['rep'=4,'fs'=4,'tp'=2] {'fs','tp'}, dimensions={0}, use_global_device_ids=true | all-gather | bytes 589824 | tf_op jit(solution)/shard_map/all_gather | solution.py:24
  31.1 0.0 copy-start.1
  31.1 0.8 copy-done.1
  31.9 0.0 copy-done.3
  31.9 0.5 convolution_multiply_fusion.1
  32.4 0.5 fusion.6
  32.9 0.0 copy-done.2
  33.0 0.0 copy-done.5
  33.0 1.5 convolution_add_fusion
  34.5 0.0 reduce-scatter.2.cloned.1.call-update
  34.5 1.8 %fusion.1 = bf16[1,2048,352]{1,2,0:T(8,128)(2,1)S(1)} fusion(bf16[128,2048]{1,0:T(8,128)(2,1)} %copy-done.1, f32[128,352]{0,1:T(8,128)} %copy-done.5, f32[128,352]{0,1:T(8,128)} %copy-done.2), kind=kOutput, calls=%fused_computation.2 | convolution fusion | flops 186261504 | bytes 2326528 | tf_op jit(solution)/shard_map/dot_general | solution.py:10
  36.3 5.7 %copy.12 = bf16[1,2048,352]{2,0,1:T(2,128)(2,1)} copy(bf16[1,2048,352]{1,2,0:T(8,128)(2,1)S(1)} %fusion.1) | data formatting | bytes 2883584 | tf_op jit(solution)/shard_map/convert_element_type | solution.py:56
  42.0 0.5 broadcast.53
  42.5 34.4 %reduce = bf16[2048,352]{1,0:T(8,128)(2,1)S(1)} reduce(bf16[2048,1,352]{2,1,0:T(2,128)(2,1)} %bitcast.16, bf16[]{:T(256)} %broadcast.53), dimensions={1}, to_apply=%bitcast.7.reduce_sub_computation | reduce | bytes 2883586
  76.9 3.6 %reshape.41 = bf16[4,2,90112]{2,1,0:T(2,128)(2,1)} reshape(bf16[2048,352]{1,0:T(8,128)(2,1)S(1)} %reduce) | data formatting | bytes 2883584
  80.5 4.9 %all-to-all-start = ((bf16[4,2,90112]{2,1,0:T(2,128)(2,1)}), bf16[4,2,90112]{2,1,0:T(2,128)(2,1)S(1)}, u32[]{:S(2)}, u32[]{:S(2)}) async-start(bf16[4,2,90112]{2,1,0:T(2,128)(2,1)} %reshape.41), calls=%async_computation.1 | async-start | bytes 2883584 | tf_op jit(solution)/shard_map/all_to_all | solution.py:55
  85.3 0.1 dynamic-slice.3
  85.4 1.1 convert_multiply_fusion
  86.5 0.0 reduce-scatter.2.cloned.1.call-done
  86.5 1.1 multiply_reduce_fusion
  87.6 51.7 %psum.7 = f32[2048]{0:T(1024)} all-reduce(f32[2048]{0:T(1024)S(1)} %get-tuple-element.3), channel_id=1, replica_groups=mesh['rep'=4,'fs'=4,'tp'=2] {'rep','fs','tp'}, use_global_device_ids=true, to_apply=%region_4.0 | all-reduce | flops 2048 | bytes 16384 | tf_op jit(solution)/shard_map/psum | solution.py:48
  139.4 1.7 %multiply_convert_fusion.6 = bf16[16,2048]{1,0:T(8,128)(2,1)} fusion(f32[16,2048]{1,0:T(8,128)} %reduce-scatter.2.cloned.1.call-done, f32[128,2048]{1,0:T(8,128)} %convert_multiply_fusion, s32[]{:T(128)S(6)} %select_n.4, f32[16]{0:T(128)S(1)} %broadcast_multiply_fusion, f32[2048]{0:T(1024)S(1)} %copy-done.7, f32[16]{0:T(128)S(1)} %dynamic-slice.3), kind=kLoop, calls=%fused_computation.17 | loop fusion | flops 163840 | bytes 336004 | tf_op jit(solution)/shard_map/convert_element_type | solution.py:52
  141.0 0.0 all-to-all-done
  141.1 4.0 %reshape.42 = bf16[2048,1,352]{2,1,0:T(2,128)(2,1)} reshape(bf16[4,2,90112]{2,1,0:T(2,128)(2,1)S(1)} %all-to-all-done) | data formatting | bytes 2883584
  145.0 7.0 %copy.13 = bf16[1,2048,352]{1,2,0:T(8,128)(2,1)S(1)} copy(bf16[1,2048,352]{2,0,1:T(2,128)(2,1)} %bitcast.17) | data formatting | bytes 2883584 | tf_op jit(solution)/shard_map/all_to_all | solution.py:55
  152.0 3.4 %reshape.40 = f32[4,512,352]{1,0,2:T(4,128)} reshape(bf16[1,2048,352]{1,2,0:T(8,128)(2,1)S(1)} %copy.13) | data formatting | bytes 4325376 | tf_op jit(solution)/shard_map/convert_element_type | solution.py:57
  155.5 4.4 %reduce_sum.39 = f32[512,352]{0,1:T(8,128)} reduce(f32[4,512,352]{1,0,2:T(4,128)} %reshape.40, f32[]{:T(128)} %constant.11.clone.1), dimensions={0}, to_apply=%region_5.0 | reduce | flops 540672 | bytes 3604484 | tf_op jit(solution)/shard_map/reduce_sum | solution.py:58
  (2 shorter events, 0.0 us)
Async XLA Ops:
  7.2 12.0 %copy-start = (bf16[2048,352]{0,1:T(8,128)(2,1)S(1)}, bf16[2048,352]{0,1:T(8,128)(2,1)}, u32[]{:S(2)}) copy-start(bf16[2048,352]{0,1:T(8,128)(2,1)} %param.9) | copy-start | bytes 4325380
  7.2 79.3 %reduce-scatter.2.cloned.1.call-start = ((), (), s32[]{:S(2)}) async-start(), calls=%async_computation.2 | async-start | bytes 1179648 | tf_op jit(solution)/shard_map/reduce_scatter | solution.py:39
  19.0 1.6 copy-start.4
  19.0 1.6 copy-start.7
  20.6 12.3 %copy-start.2 = (f32[128,352]{0,1:T(8,128)}, f32[128,352]{0,1:T(8,128)S(1)}, u32[]{:S(2)}) copy-start(f32[128,352]{0,1:T(8,128)S(1)} %fusion.3) | copy-start | bytes 540676
  20.6 0.9 copy-start.6
  20.7 11.2 %copy-start.3 = (bf16[352,2048]{1,0:T(8,128)(2,1)S(1)}, bf16[352,2048]{1,0:T(8,128)(2,1)}, u32[]{:S(2)}) copy-start(bf16[352,2048]{1,0:T(8,128)(2,1)} %param.11) | copy-start | bytes 4325380
  21.6 11.4 %copy-start.5 = (f32[128,352]{0,1:T(8,128)}, f32[128,352]{0,1:T(8,128)S(1)}, u32[]{:S(2)}) copy-start(f32[128,352]{0,1:T(8,128)S(1)} %fusion.4) | copy-start | bytes 540676
  31.1 0.8 copy-start.1
  80.5 60.6 %all-to-all-start = ((bf16[4,2,90112]{2,1,0:T(2,128)(2,1)}), bf16[4,2,90112]{2,1,0:T(2,128)(2,1)S(1)}, u32[]{:S(2)}, u32[]{:S(2)}) async-start(bf16[4,2,90112]{2,1,0:T(2,128)(2,1)} %reshape.41), calls=%async_computation.1 | async-start | bytes 2883584 | tf_op jit(solution)/shard_map/all_to_all | solution.py:55
Sparse Core Ops, SparseCore 0:
  34.6 36.2 reduce-scatter.1
where the time goes:
time: 167 us
  blocking collectives  73 us (44%)
  other arithmetic  42.9 us (26%)
  local copies, waits for them, and re-layouts  25.4 us (15%)
  between operations  14.2 us (9%)
  matrix products  6.35 us (4%)
  starting transfers between devices  4.91 us (3%)
    psum x1, blocking collectives, per_device(): lax.psum(jnp.sum(d_in * own_normed, axis=0), ('rep', 'fs', 'tp'))  51.7 us
    unnamed x1, other arithmetic  34.4 us
    all_gather x1, blocking collectives, per_device(): lax.all_gather(inputs, ('fs', 'tp'), axis=0, tiled=True)  11.8 us
    all_gather x1, blocking collectives, per_device(): lax.all_gather(cotangent, ('fs', 'tp'), axis=0, tiled=True)  9.52 us
    unnamed x19, local copies, waits for them, and re-layouts  9.19 us
    all_to_all x1, local copies, waits for them, and re-layouts, per_device(): lax.all_to_all(part_down[None].astype(jnp.bfloat16), 'rep', split_axis=1,...  7.01 us
    convert_element_type x1, local copies, waits for them, and re-layouts, per_device(): part_down[None].astype(jnp.bfloat16)  5.72 us
    all_to_all x1, starting transfers between devices, per_device(): lax.all_to_all(part_down[None].astype(jnp.bfloat16), 'rep', split_axis=1,...  4.87 us
  transfers between devices with their start and end apart: 2, of which 0 were waited for; matrix products, arithmetic and copies ran while one was open for 30% of the time, Pallas kernels for 0%

commit v1 on v0

--- a/solution.py
+++ b/solution.py
@@ -45,7 +45,7 @@
     offset = lax.axis_index(("fs", "tp")) * own_rows
     own_normed = lax.dynamic_slice_in_dim(normed, offset, own_rows, 0)
     own_inv = lax.dynamic_slice_in_dim(inv, offset, own_rows, 0)
-    gain_grad = lax.psum(jnp.sum(d_in * own_normed, axis=0), ("rep", "fs", "tp"))
+    gain_grad = lax.psum(lax.psum(jnp.sum(d_in * own_normed, axis=0), "rep"), ("fs", "tp"))
     scaled = d_in * norm_gain
     input_grad = (
         own_inv * (scaled - own_normed * jnp.mean(scaled * own_normed, axis=-1, keepdims=True))

time: 167 us -> 161 us (0.964)
  the two profiles are of different devices: /device:TPU:0 before, /device:TPU:16 now
where the time goes in v1:
time: 161 us; the launch traced here: 160 us
  blocking collectives  66.3 us (41%)
  other arithmetic  42.8 us (27%)
  local copies, waits for them, and re-layouts  25.4 us (16%)
  between operations  14.2 us (9%)
  matrix products  6.35 us (4%)
  starting transfers between devices  5.24 us (3%)
    unnamed x1, other arithmetic  34.4 us
    psum x1, blocking collectives, per_device(): lax.psum(jnp.sum(d_in * own_normed, axis=0), 'rep')  33.7 us
    psum x1, blocking collectives, per_device(): lax.psum(lax.psum(jnp.sum(d_in * own_normed, axis=0), 'rep'), ('fs', 'tp'))  12.8 us
    all_gather x1, blocking collectives, per_device(): lax.all_gather(inputs, ('fs', 'tp'), axis=0, tiled=True)  10.3 us
    all_gather x1, blocking collectives, per_device(): lax.all_gather(cotangent, ('fs', 'tp'), axis=0, tiled=True)  9.52 us
    unnamed x19, local copies, waits for them, and re-layouts  9.19 us
    all_to_all x1, local copies, waits for them, and re-layouts, per_device(): lax.all_to_all(part_down[None].astype(jnp.bfloat16), 'rep', split_axis=1,...  7.01 us
    convert_element_type x1, local copies, waits for them, and re-layouts, per_device(): part_down[None].astype(jnp.bfloat16)  5.72 us
  transfers between devices with their start and end apart: 2, of which 0 were waited for; matrix products, arithmetic and copies ran while one was open for 31% of the time, Pallas kernels for 0%

profile of v1, /device:TPU:16, one launch (start us, length us, event | category | flops | bytes accessed | tf_op | source)
XLA Modules:
  0.0 160.3 jit_solution(4573061655616328672)
XLA Ops:
  7.2 0.0 copy-start
  7.2 0.0 reduce-scatter.2.cloned.1.call-start
  7.2 10.3 %all_gather.6 = bf16[128,2048]{1,0:T(8,128)(2,1)S(1)} all-gather(bf16[16,2048]{1,0:T(8,128)(2,1)} %param.6), channel_id=1, replica_groups=mesh['rep'=4,'fs'=4,'tp'=2] {'fs','tp'}, dimensions={0}, use_global_device_ids=true | all-gather | bytes 589824 | tf_op jit(solution)/shard_map/all_gather | solution.py:23
  17.5 0.0 copy-start.4
  17.5 0.0 copy-start.7
  17.5 0.2 fusion.2
  17.7 0.0 copy-done
  17.7 1.4 fusion.3
  19.1 0.0 copy-done.4
  19.1 0.0 copy-done.7
  19.2 0.0 copy-start.2
  19.2 0.0 copy-start.6
  19.2 0.0 copy-start.3
  19.2 0.6 fusion.4
  19.8 0.3 copy-done.6
  20.1 0.0 copy-start.5
  20.1 9.5 %all_gather.7 = bf16[128,2048]{1,0:T(8,128)(2,1)S(1)} all-gather(bf16[16,2048]{1,0:T(8,128)(2,1)S(1)} %copy-done.6), channel_id=1, replica_groups=mesh['rep'=4,'fs'=4,'tp'=2] {'fs','tp'}, dimensions={0}, use_global_device_ids=true | all-gather | bytes 589824 | tf_op jit(solution)/shard_map/all_gather | solution.py:24
  29.6 0.0 copy-start.1
  29.6 0.8 copy-done.1
  30.4 0.0 copy-done.3
  30.4 0.5 convolution_multiply_fusion.1
  30.9 0.5 fusion.6
  31.5 0.0 copy-done.2
  31.5 0.0 copy-done.5
  31.5 1.5 convolution_add_fusion
  33.0 0.0 reduce-scatter.2.cloned.1.call-update
  33.0 1.8 %fusion.1 = bf16[1,2048,352]{1,2,0:T(8,128)(2,1)S(1)} fusion(bf16[128,2048]{1,0:T(8,128)(2,1)} %copy-done.1, f32[128,352]{0,1:T(8,128)} %copy-done.5, f32[128,352]{0,1:T(8,128)} %copy-done.2), kind=kOutput, calls=%fused_computation.2 | convolution fusion | flops 186261504 | bytes 2326528 | tf_op jit(solution)/shard_map/dot_general | solution.py:10
  34.8 5.7 %copy.12 = bf16[1,2048,352]{2,0,1:T(2,128)(2,1)} copy(bf16[1,2048,352]{1,2,0:T(8,128)(2,1)S(1)} %fusion.1) | data formatting | bytes 2883584 | tf_op jit(solution)/shard_map/convert_element_type | solution.py:56
  40.5 0.5 broadcast.53
  41.0 34.4 %reduce = bf16[2048,352]{1,0:T(8,128)(2,1)S(1)} reduce(bf16[2048,1,352]{2,1,0:T(2,128)(2,1)} %bitcast.16, bf16[]{:T(256)} %broadcast.53), dimensions={1}, to_apply=%bitcast.7.reduce_sub_computation | reduce | bytes 2883586
  75.4 3.6 %reshape.41 = bf16[4,2,90112]{2,1,0:T(2,128)(2,1)} reshape(bf16[2048,352]{1,0:T(8,128)(2,1)S(1)} %reduce) | data formatting | bytes 2883584
  79.0 5.2 %all-to-all-start = ((bf16[4,2,90112]{2,1,0:T(2,128)(2,1)}), bf16[4,2,90112]{2,1,0:T(2,128)(2,1)S(1)}, u32[]{:S(2)}, u32[]{:S(2)}) async-start(bf16[4,2,90112]{2,1,0:T(2,128)(2,1)} %reshape.41), calls=%async_computation.1 | async-start | bytes 2883584 | tf_op jit(solution)/shard_map/all_to_all | solution.py:55
  84.2 0.1 dynamic-slice.3
  84.3 1.1 convert_multiply_fusion
  85.4 0.0 reduce-scatter.2.cloned.1.call-done
  85.4 1.1 multiply_reduce_fusion
  86.5 33.7 %psum.14 = f32[2048]{0:T(1024)S(1)} all-reduce(f32[2048]{0:T(1024)S(1)} %get-tuple-element.3), channel_id=1, replica_groups=mesh['rep'=4,'fs'=4,'tp'=2] {'rep'}, use_global_device_ids=true, to_apply=%region_4.0 | all-reduce | flops 2048 | bytes 16384 | tf_op jit(solution)/shard_map/psum | solution.py:48
  120.2 12.8 %psum.15 = f32[2048]{0:T(1024)} all-reduce(f32[2048]{0:T(1024)S(1)} %psum.14), channel_id=1, replica_groups=mesh['rep'=4,'fs'=4,'tp'=2] {'fs','tp'}, use_global_device_ids=true, to_apply=%region_5.0 | all-reduce | flops 2048 | bytes 16384 | tf_op jit(solution)/shard_map/psum | solution.py:48
  133.0 1.7 %multiply_convert_fusion.6 = bf16[16,2048]{1,0:T(8,128)(2,1)} fusion(f32[16,2048]{1,0:T(8,128)} %reduce-scatter.2.cloned.1.call-done, f32[128,2048]{1,0:T(8,128)} %convert_multiply_fusion, s32[]{:T(128)S(6)} %select_n.4, f32[16]{0:T(128)S(1)} %broadcast_multiply_fusion, f32[2048]{0:T(1024)S(1)} %copy-done.7, f32[16]{0:T(128)S(1)} %dynamic-slice.3), kind=kLoop, calls=%fused_computation.17 | loop fusion | flops 163840 | bytes 336004 | tf_op jit(solution)/shard_map/convert_element_type | solution.py:52
  134.7 0.0 all-to-all-done
  134.7 4.0 %reshape.42 = bf16[2048,1,352]{2,1,0:T(2,128)(2,1)} reshape(bf16[4,2,90112]{2,1,0:T(2,128)(2,1)S(1)} %all-to-all-done) | data formatting | bytes 2883584
  138.6 7.0 %copy.13 = bf16[1,2048,352]{1,2,0:T(8,128)(2,1)S(1)} copy(bf16[1,2048,352]{2,0,1:T(2,128)(2,1)} %bitcast.17) | data formatting | bytes 2883584 | tf_op jit(solution)/shard_map/all_to_all | solution.py:55
  145.7 3.4 %reshape.40 = f32[4,512,352]{1,0,2:T(4,128)} reshape(bf16[1,2048,352]{1,2,0:T(8,128)(2,1)S(1)} %copy.13) | data formatting | bytes 4325376 | tf_op jit(solution)/shard_map/convert_element_type | solution.py:57
  149.1 4.4 %reduce_sum.39 = f32[512,352]{0,1:T(8,128)} reduce(f32[4,512,352]{1,0,2:T(4,128)} %reshape.40, f32[]{:T(128)} %constant.11.clone.1), dimensions={0}, to_apply=%region_6.0 | reduce | flops 540672 | bytes 3604484 | tf_op jit(solution)/shard_map/reduce_sum | solution.py:58
  (2 shorter events, 0.0 us)
Async XLA Ops:
  7.2 10.6 %copy-start = (bf16[2048,352]{0,1:T(8,128)(2,1)S(1)}, bf16[2048,352]{0,1:T(8,128)(2,1)}, u32[]{:S(2)}) copy-start(bf16[2048,352]{0,1:T(8,128)(2,1)} %param.9) | copy-start | bytes 4325380
  7.2 78.2 %reduce-scatter.2.cloned.1.call-start = ((), (), s32[]{:S(2)}) async-start(), calls=%async_computation.2 | async-start | bytes 1179648 | tf_op jit(solution)/shard_map/reduce_scatter | solution.py:39
  17.5 1.6 %copy-start.4 = (bf16[2048,352]{0,1:T(8,128)(2,1)S(1)}, bf16[2048,352]{0,1:T(8,128)(2,1)}, u32[]{:S(2)}) copy-start(bf16[2048,352]{0,1:T(8,128)(2,1)} %param.10) | copy-start | bytes 4325380
  17.5 1.6 %copy-start.7 = (f32[2048]{0:T(1024)S(1)}, f32[2048]{0:T(1024)}, u32[]{:S(2)}) copy-start(f32[2048]{0:T(1024)} %param.8) | copy-start | bytes 24580
  19.2 12.3 %copy-start.2 = (f32[128,352]{0,1:T(8,128)}, f32[128,352]{0,1:T(8,128)S(1)}, u32[]{:S(2)}) copy-start(f32[128,352]{0,1:T(8,128)S(1)} %fusion.3) | copy-start | bytes 540676
  19.2 0.9 copy-start.6
  19.2 11.2 %copy-start.3 = (bf16[352,2048]{1,0:T(8,128)(2,1)S(1)}, bf16[352,2048]{1,0:T(8,128)(2,1)}, u32[]{:S(2)}) copy-start(bf16[352,2048]{1,0:T(8,128)(2,1)} %param.11) | copy-start | bytes 4325380
  20.1 11.4 %copy-start.5 = (f32[128,352]{0,1:T(8,128)}, f32[128,352]{0,1:T(8,128)S(1)}, u32[]{:S(2)}) copy-start(f32[128,352]{0,1:T(8,128)S(1)} %fusion.4) | copy-start | bytes 540676
  29.6 0.8 copy-start.1
  79.0 55.7 %all-to-all-start = ((bf16[4,2,90112]{2,1,0:T(2,128)(2,1)}), bf16[4,2,90112]{2,1,0:T(2,128)(2,1)S(1)}, u32[]{:S(2)}, u32[]{:S(2)}) async-start(bf16[4,2,90112]{2,1,0:T(2,128)(2,1)} %reshape.41), calls=%async_computation.1 | async-start | bytes 2883584 | tf_op jit(solution)/shard_map/all_to_all | solution.py:55
Sparse Core Ops, SparseCore 0:
  33.1 36.0 reduce-scatter.1
